TPU v7x, 32 devices: a whole 2x2x4 slice. The times are simulated.
32 devices in a mesh: ep: 8 (over z, core), tp: 4 (over y, x).
Axes of the slice: x: 2, y: 2, z: 4, core: 2. Of those that a mesh axis runs over, the one named last changes fastest.
Arguments:
- tokens: bfloat16 [256, 2560], P('ep'), may hold values from -6 to 6
- norm_gain: float32 [2560], replicated, may hold values from 0.1 to 1.9
- route: int32 [256, 4], P('ep'), may hold values from 0 to 7, all different within a row; in each aligned block of 32 rows (0 to 31, 32 to 63, ...) at most 24 rows name the same one
- route_weight: float32 [256, 4], P('ep'), may hold values from 0.1 to 1
- gate_weight: bfloat16 [8, 8960, 2560], P('ep', 'tp'), may hold values from -0.125 to 0.125
- up_weight: bfloat16 [8, 8960, 2560], P('ep', 'tp'), may hold values from -0.125 to 0.125
- down_weight: bfloat16 [8, 8960, 2560], P('ep', 'tp'), may hold values from -0.0625 to 0.0625
Outputs:
- mixed: bfloat16 [256, 2560], P('ep', 'tp')
Inputs may be any that keep to these rules, and one draw needn't show every extreme that they name: `route`: each row names 4 different experts. Among the rows of one index of ep no expert is named more than 24 times, a bound that some block reaches.
All inputs are finite; a program needn't handle non-finite values.
Results may differ from a plain program's by a relative error of at most 0.018.
Values may be sent and summed in bfloat16 or wider, within the bound.
A program may use at most 128 MiB of HBM per device.

v0:
```python
import jax
import jax.numpy as jnp
from jax import lax
from jax.sharding import PartitionSpec as P

epsilon = 1e-06


def on_device(tokens, norm_gain, route, route_weight, gate_weight, up_weight, down_weight):
    tok_rows, width = tokens.shape
    top_count = route.shape[1]
    local_experts = gate_weight.shape[0]
    ep_count = lax.axis_size("ep")
    tp_count = lax.axis_size("tp")
    experts = local_experts * ep_count
    capacity = min(tok_rows, max(2, (3 * tok_rows * top_count + 2 * experts - 1) // (2 * experts)))
    width_share = width // tp_count
    values = tokens.astype(jnp.float32)
    scaled = values * lax.rsqrt(jnp.mean(values * values, axis=-1, keepdims=True) + epsilon)
    normed = (scaled * norm_gain).astype(jnp.bfloat16)
    flat_route = route.reshape(tok_rows * top_count)
    onehot = (flat_route[:, None] == jnp.arange(experts, dtype=jnp.int32)[None, :]).astype(
        jnp.int32
    )
    slot_number = jnp.sum((jnp.cumsum(onehot, axis=0) - 1) * onehot, axis=-1)
    slot_index = flat_route * capacity + slot_number
    placing = (
        slot_index[None, :] == jnp.arange(experts * capacity, dtype=jnp.int32)[:, None]
    ).astype(jnp.bfloat16)
    repeated = jnp.repeat(normed, top_count, axis=0)
    columns = lax.dynamic_slice_in_dim(repeated, lax.axis_index("tp") * width_share, width_share, 1)
    send = jnp.dot(placing, columns, preferred_element_type=jnp.float32).astype(jnp.bfloat16)
    send = send.reshape(ep_count, local_experts, capacity, width_share)
    arrived = lax.all_to_all(send, "ep", split_axis=0, concat_axis=0, tiled=True)
    piece = lax.all_gather(arrived, "tp", axis=3, tiled=True)
    gate = jnp.einsum("sjcd,jfd->sjcf", piece, gate_weight, preferred_element_type=jnp.float32)
    upward = jnp.einsum("sjcd,jfd->sjcf", piece, up_weight, preferred_element_type=jnp.float32)
    hidden = (jax.nn.silu(gate) * upward).astype(jnp.bfloat16)
    partial_value = jnp.einsum(
        "sjcf,jfd->sjcd", hidden, down_weight, preferred_element_type=jnp.float32
    )
    shares = lax.psum_scatter(
        partial_value.astype(jnp.bfloat16), "tp", scatter_dimension=3, tiled=True
    )
    returned = lax.all_to_all(shares, "ep", split_axis=0, concat_axis=0, tiled=True)
    results = returned.reshape(experts * capacity, width_share)
    picked = results[slot_index].reshape(tok_rows, top_count, width_share).astype(jnp.float32)
    mixed = jnp.sum(route_weight[:, :, None] * picked, axis=1)
    return mixed.astype(jnp.bfloat16)


def solution(mesh):
    placed = (
        P("ep", None),
        P(),
        P("ep", None),
        P("ep", None),
        P("ep", "tp", None),
        P("ep", "tp", None),
        P("ep", "tp", None),
    )
    return jax.shard_map(
        on_device, mesh=mesh, in_specs=placed, out_specs=P("ep", "tp"), check_vma=False
    )
```

profile of v0, /device:TPU:0, one launch (start us, length us, event | category | flops | bytes accessed | tf_op | source)
XLA Modules:
  0.0 130.7 jit_solution(8233798995752015378)
XLA Ops:
  6.5 0.8 copy.15
  7.3 0.1 reshape.82
  7.4 0.1 fusion.37
  7.5 0.2 reduce_window_sum.11
  7.7 0.2 select_reduce_fusion
  7.9 1.1 fusion.33
  8.9 1.0 fusion.35
  10.0 0.2 broadcast_in_dim.2
  10.1 0.1 reshape.83
  10.3 0.2 convolution_convert_fusion
  10.5 15.5 %all_to_all.10 = bf16[8,1,24,640]{3,2,1,0:T(8,128)(2,1)S(1)} all-to-all(bf16[8,1,24,640]{3,2,1,0:T(8,128)(2,1)S(1)} %bitcast.85), channel_id=1, replica_groups=mesh['ep'=8,'tp'=4] {'ep'}, dimensions={0} | all-to-all | bytes 491520 | tf_op jit(solution)/shard_map/all_to_all | solution.py:34
  26.0 13.9 %all_gather.3 = bf16[8,1,24,2560]{3,2,0,1:T(8,128)(2,1)S(1)} all-gather(bf16[8,1,24,640]{3,2,0,1:T(8,128)(2,1)S(1)} %bitcast.84), channel_id=1, replica_groups=mesh['ep'=8,'tp'=4] {'tp'}, dimensions={3}, use_global_device_ids=true | all-gather | bytes 1228800 | tf_op jit(solution)/shard_map/all_gather | solution.py:35
  39.9 9.2 %fusion.6 = f32[8,1,24,2240]{3,2,0,1:T(8,128)} fusion(bf16[1,2240,2560]{2,1,0:T(8,128)(2,1)} %param.11, bf16[8,1,24,2560]{3,2,0,1:T(8,128)(2,1)S(1)} %all_gather.3), kind=kOutput, calls=%fused_computation.7 | convolution fusion | flops 2202009600 | bytes 14172160 | tf_op jit(solution)/shard_map/sjcd,jfd->sjcf/dot_general | solution.py:36
  49.1 14.7 %fusion.24 = bf16[8,1,24,2560]{3,2,0,1:T(8,128)(2,1)S(1)} fusion(bf16[1,2240,2560]{2,1,0:T(8,128)(2,1)} %param.13, bf16[1,2240,2560]{2,1,0:T(8,128)(2,1)} %param.12, f32[8,1,24,2240]{3,2,0,1:T(8,128)} %fusion.6, bf16[8,1,24,2560]{3,2,0,1:T(8,128)(2,1)S(1)} %all_gather.3), kind=kOutput, calls=%fused_computation.13 | convolution fusion | flops 4407091200 | bytes 26624000 | tf_op jit(solution)/shard_map/sjcf,jfd->sjcd/dot_general | solution.py:39
  63.8 4.6 %copy.20 = bf16[8,1,24,2560]{2,0,1,3:T(8,128)(2,1)} copy(bf16[8,1,24,2560]{3,2,0,1:T(8,128)(2,1)S(1)} %fusion.24) | data formatting | bytes 1966080
  68.4 7.3 %reshape.103 = bf16[2560,192]{1,0:T(8,128)(2,1)} reshape(bf16[2560,1,8,24]{3,2,1,0:T(8,128)(2,1)} %bitcast.81) | data formatting | bytes 1966080
  75.7 28.7 %reduce-scatter.4.cloned.1.call-done = bf16[640,192]{1,0:T(8,128)(2,1)} async-done(((bf16[2560,192]{1,0:T(8,128)(2,1)}), bf16[640,192]{1,0:T(8,128)(2,1)}) %reduce-scatter.4.cloned.1.call-update) | async-done | bytes 245776
  104.5 2.0 %reshape.104 = bf16[640,1,8,24]{3,2,1,0:T(8,128)(2,1)S(1)} reshape(bf16[640,192]{1,0:T(8,128)(2,1)} %reduce-scatter.4.cloned.1.call-done) | data formatting | bytes 491520
  106.5 1.5 %copy.21 = bf16[8,1,24,640]{3,2,0,1:T(8,128)(2,1)} copy(bf16[8,1,24,640]{2,0,1,3:T(8,128)(2,1)S(1)} %bitcast.83) | data formatting | bytes 491520
  108.0 4.6 %all-to-all-start.1 = ((bf16[8,1,24,640]{3,2,1,0:T(8,128)(2,1)}), bf16[8,1,24,640]{3,2,1,0:T(8,128)(2,1)S(1)}, u32[]{:S(2)}, u32[]{:S(2)}) async-start(bf16[8,1,24,640]{3,2,1,0:T(8,128)(2,1)} %bitcast.22), calls=%async_computation.1 | async-start | bytes 491520 | tf_op jit(solution)/shard_map/all_to_all | solution.py:45
  112.7 0.1 mul.78
  112.9 9.0 %all-to-all-done.1 = bf16[8,1,24,640]{3,2,1,0:T(8,128)(2,1)S(1)} async-done(((bf16[8,1,24,640]{3,2,1,0:T(8,128)(2,1)}), bf16[8,1,24,640]{3,2,1,0:T(8,128)(2,1)S(1)}, u32[]{:S(2)}, u32[]{:S(2)}) %all-to-all-start.1) | async-done | bytes 245792 | tf_op jit(solution)/shard_map/all_to_all | solution.py:45
  121.9 0.9 gather_fusion
  122.9 0.9 multiply_reduce_fusion
  (14 shorter events, 0.3 us)
Async XLA Ops:
  6.5 97.9 %reduce-scatter.4.cloned.1.call-start = ((), (), s32[]{:S(2)}) async-start(), calls=%async_computation.3 | async-start | bytes 1638400
  75.7 36.9 %copy-start = (s32[32,4]{0,1:T(4,128)S(1)}, s32[32,4]{0,1:T(4,128)}, u32[]{:S(2)}) copy-start(s32[32,4]{0,1:T(4,128)} %param.9) | copy-start | bytes 1540
  75.7 37.1 %copy-start.1 = (f32[32,4]{0,1:T(4,128)S(1)}, f32[32,4]{0,1:T(4,128)}, u32[]{:S(2)}) copy-start(f32[32,4]{0,1:T(4,128)} %param.10) | copy-start | bytes 1540
  108.0 14.0 %all-to-all-start.1 = ((bf16[8,1,24,640]{3,2,1,0:T(8,128)(2,1)}), bf16[8,1,24,640]{3,2,1,0:T(8,128)(2,1)S(1)}, u32[]{:S(2)}, u32[]{:S(2)}) async-start(bf16[8,1,24,640]{3,2,1,0:T(8,128)(2,1)} %bitcast.22), calls=%async_computation.1 | async-start | bytes 491520 | tf_op jit(solution)/shard_map/all_to_all | solution.py:45
Sparse Core Ops, SparseCore 0:
  75.8 28.5 reduce-scatter.3
where the time goes:
time: 131 us
  waiting for transfers between devices  37.8 us (29%)
  blocking collectives  29.4 us (22%)
  matrix products  24.1 us (18%)
  local copies, waits for them, and re-layouts  17.8 us (14%)
  between operations  13.5 us (10%)
  starting transfers between devices  4.61 us (4%)
  other arithmetic  3.44 us (3%)
    unnamed x2, waiting for transfers between devices  28.8 us
    unnamed x10, local copies, waits for them, and re-layouts  16.2 us
    all_to_all x1, blocking collectives, on_device(): lax.all_to_all(send, 'ep', split_axis=0, concat_axis=0, tiled=True)  15.5 us
    dot_general x1, matrix products, on_device(): jnp.einsum('sjcf,jfd->sjcd', hidden, down_weight, preferred_element_type=...  14.7 us
    all_gather x1, blocking collectives, on_device(): piece = lax.all_gather(arrived, 'tp', axis=3, tiled=True)  13.9 us
    dot_general x1, matrix products, on_device(): jnp.einsum('sjcd,jfd->sjcf', piece, gate_weight, preferred_element_type=j...  9.21 us
    all_to_all x1, waiting for transfers between devices, on_device(): lax.all_to_all(shares, 'ep', split_axis=0, concat_axis=0, tiled=True)  9.04 us
    all_to_all x1, starting transfers between devices, on_device(): lax.all_to_all(shares, 'ep', split_axis=0, concat_axis=0, tiled=True)  4.6 us
  transfers between devices with their start and end apart: 2, of which 2 were waited for; matrix products, arithmetic and copies ran while one was open for 0% of the time, Pallas kernels for 0%

commit v1 on v0

--- a/solution.py
+++ b/solution.py
@@ -4,6 +4,28 @@
 from jax.sharding import PartitionSpec as P
 
 epsilon = 1e-06
+
+
+def in_blocks(array, dim, peers):
+    before, after = (array.shape[:dim], array.shape[dim + 1 :])
+    return jnp.moveaxis(array.reshape(*before, peers, -1, *after), dim, 0)
+
+
+def joined_along(tiles, dim):
+    tiles = jnp.moveaxis(tiles, 0, dim)
+    lengths = tiles.shape
+    return tiles.reshape(*lengths[:dim], lengths[dim] * lengths[dim + 1], *lengths[dim + 2 :])
+
+
+def swapped_with_each(value, axis, split_dim, concat_dim):
+    size, place = (lax.axis_size(axis), lax.axis_index(axis))
+    blocks = in_blocks(value, split_dim, size)
+    outs = [blocks[place]]
+    for step in range(1, size):
+        sent = blocks[place ^ step]
+        outs.append(lax.ppermute(sent, axis, [(i, i ^ step) for i in range(size)]))
+    blocks = jnp.stack(outs)[place ^ jnp.arange(size)]
+    return joined_along(blocks, concat_dim)
 
 
 def on_device(tokens, norm_gain, route, route_weight, gate_weight, up_weight, down_weight):
@@ -31,7 +53,7 @@
     columns = lax.dynamic_slice_in_dim(repeated, lax.axis_index("tp") * width_share, width_share, 1)
     send = jnp.dot(placing, columns, preferred_element_type=jnp.float32).astype(jnp.bfloat16)
     send = send.reshape(ep_count, local_experts, capacity, width_share)
-    arrived = lax.all_to_all(send, "ep", split_axis=0, concat_axis=0, tiled=True)
+    arrived = swapped_with_each(send, "ep", 0, 0)
     piece = lax.all_gather(arrived, "tp", axis=3, tiled=True)
     gate = jnp.einsum("sjcd,jfd->sjcf", piece, gate_weight, preferred_element_type=jnp.float32)
     upward = jnp.einsum("sjcd,jfd->sjcf", piece, up_weight, preferred_element_type=jnp.float32)

time: 131 us -> 131 us (level)
  blocking collectives: 29.4 us -> 15.2 us
  starting transfers between devices: 4.61 us -> 14.4 us
  waiting for transfers between devices: 37.8 us -> 41 us
    all_to_all x1 -> x0, blocking collectives: 15.5 us -> none  [on_device(): lax.all_to_all(send, 'ep', split_axis=0, concat_axis=0, tiled=True)]
    ppermute x0 -> x7, starting transfers between devices: none -> 9.8 us  [swapped_with_each(): outs.append(lax.ppermute(sent, axis, [(i, i ^ step) for i in range(size)]))]
    ppermute x0 -> x7, waiting for transfers between devices: none -> 4.99 us  [swapped_with_each(): outs.append(lax.ppermute(sent, axis, [(i, i ^ step) for i in range(size)]))]
    unnamed x2, waiting for transfers between devices: 28.8 us -> 27 us
    all_gather x1, blocking collectives: 13.9 us -> 15.2 us  [on_device(): piece = lax.all_gather(arrived, 'tp', axis=3, tiled=True)]
    unnamed x10 -> x16, local copies, waits for them, and re-layouts: 16.2 us -> 16.3 us
  transfers between devices with their start and end apart: 2 -> 9, of which waited for: 2 -> 5; matrix products, arithmetic and copies ran while one was open for 0% -> 0% of each run, Pallas kernels for 0% -> 0%
where the time goes in v1:
time: 131 us; the launch traced here: 130 us
  waiting for transfers between devices  41 us (31%)
  matrix products  24.1 us (18%)
  local copies, waits for them, and re-layouts  18.5 us (14%)
  blocking collectives  15.2 us (12%)
  starting transfers between devices  14.4 us (11%)
  between operations  13.6 us (10%)
  other arithmetic  3.45 us (3%)
    unnamed x2, waiting for transfers between devices  27 us
    unnamed x16, local copies, waits for them, and re-layouts  16.3 us
    all_gather x1, blocking collectives, on_device(): piece = lax.all_gather(arrived, 'tp', axis=3, tiled=True)  15.2 us
    dot_general x1, matrix products, on_device(): jnp.einsum('sjcf,jfd->sjcd', hidden, down_weight, preferred_element_type=...  14.7 us
    ppermute x7, starting transfers between devices, swapped_with_each(): outs.append(lax.ppermute(sent, axis, [(i, i ^ step) for i in range(size)]))  9.8 us
    dot_general x1, matrix products, on_device(): jnp.einsum('sjcd,jfd->sjcf', piece, gate_weight, preferred_element_type=j...  9.22 us
    all_to_all x1, waiting for transfers between devices, on_device(): lax.all_to_all(shares, 'ep', split_axis=0, concat_axis=0, tiled=True)  9.04 us
    ppermute x7, waiting for transfers between devices, swapped_with_each(): outs.append(lax.ppermute(sent, axis, [(i, i ^ step) for i in range(size)]))  4.99 us
  transfers between devices with their start and end apart: 9, of which 5 were waited for; matrix products, arithmetic and copies ran while one was open for 0% of the time, Pallas kernels for 0%

profile of v1, /device:TPU:0, one launch (start us, length us, event | category | flops | bytes accessed | tf_op | source)
XLA Modules:
  0.0 130.4 jit_solution(8765678444650808613)
XLA Ops:
  6.5 0.8 copy.15
  7.9 1.1 fusion.30
  8.9 1.0 fusion.32
  10.3 0.2 convolution_convert_fusion
  10.6 0.6 collective-permute-start
  11.2 2.6 %collective-permute-start.1 = (bf16[1,1,24,640]{3,2,1,0:T(8,128)(2,1)S(1)}, bf16[1,1,24,640]{3,2,1,0:T(8,128)(2,1)S(1)}, u32[]{:S(2)}, u32[]{:S(2)}) collective-permute-start(bf16[1,1,24,640]{3,2,1,0:T(8,128)(2,1)S(1)} %get-tuple-element.10), channel_id=1, source_target_pairs={{0,8},{4,12},{8,0},{12,4},{16,24},{20,28},{24,16},{28,20},{1,9},{5... | collective-permute-start | bytes 92168 | tf_op jit(solution)/shard_map/ppermute | solution.py:26
  13.8 2.8 %collective-permute-start.3 = (bf16[1,1,24,640]{3,2,1,0:T(8,128)(2,1)S(1)}, bf16[1,1,24,640]{3,2,1,0:T(8,128)(2,1)S(1)}, u32[]{:S(2)}, u32[]{:S(2)}) collective-permute-start(bf16[1,1,24,640]{3,2,1,0:T(8,128)(2,1)S(1)} %get-tuple-element.8), channel_id=1, source_target_pairs={{0,16},{4,20},{8,24},{12,28},{16,0},{20,4},{24,8},{28,12},{1,17},{... | collective-permute-start | bytes 92168 | tf_op jit(solution)/shard_map/ppermute | solution.py:26
  16.6 3.7 %collective-permute-start.5 = (bf16[1,1,24,640]{3,2,1,0:T(8,128)(2,1)S(1)}, bf16[1,1,24,640]{3,2,1,0:T(8,128)(2,1)S(1)}, u32[]{:S(2)}, u32[]{:S(2)}) collective-permute-start(bf16[1,1,24,640]{3,2,1,0:T(8,128)(2,1)S(1)} %get-tuple-element.6), channel_id=1, source_target_pairs={{0,24},{4,28},{8,16},{12,20},{16,8},{20,12},{24,0},{28,4},{1,25},{... | collective-permute-start | bytes 92168 | tf_op jit(solution)/shard_map/ppermute | solution.py:26
  20.5 0.4 collective-permute-done.4
  20.9 2.0 %collective-permute-done.5 = bf16[1,1,24,640]{3,2,1,0:T(8,128)(2,1)S(1)} collective-permute-done((bf16[1,1,24,640]{3,2,1,0:T(8,128)(2,1)S(1)}, bf16[1,1,24,640]{3,2,1,0:T(8,128)(2,1)S(1)}, u32[]{:S(2)}, u32[]{:S(2)}) %collective-permute-start.5) | collective-permute-done | bytes 30752 | tf_op jit(solution)/shard_map/ppermute | solution.py:26
  22.9 2.6 %collective-permute-done.6 = bf16[1,1,24,640]{3,2,1,0:T(8,128)(2,1)S(1)} collective-permute-done((bf16[1,1,24,640]{3,2,1,0:T(8,128)(2,1)S(1)}, bf16[1,1,24,640]{3,2,1,0:T(8,128)(2,1)S(1)}, u32[]{:S(2)}, u32[]{:S(2)}) %collective-permute-start.6) | collective-permute-done | bytes 30752 | tf_op jit(solution)/shard_map/ppermute | solution.py:26
  25.5 0.6 gather_fusion
  26.1 15.2 %all-gather = bf16[8,24,2560]{2,1,0:T(8,128)(2,1)S(1)} all-gather(bf16[8,24,640]{2,1,0:T(8,128)(2,1)S(1)} %gather_fusion), channel_id=2, replica_groups=mesh['ep'=8,'tp'=4] {'tp'}, dimensions={2}, use_global_device_ids=true | all-gather | bytes 1228800 | tf_op jit(solution)/shard_map/all_gather | solution.py:57
  41.3 9.2 %fusion.6 = f32[8,1,24,2240]{3,2,0,1:T(8,128)} fusion(bf16[8,24,2560]{2,1,0:T(8,128)(2,1)S(1)} %all-gather, bf16[1,2240,2560]{2,1,0:T(8,128)(2,1)} %param.11), kind=kOutput, calls=%fused_computation.8 | convolution fusion | flops 2202009600 | bytes 14172160 | tf_op jit(solution)/shard_map/sjcd,jfd->sjcf/dot_general | solution.py:58
  50.5 14.7 %fusion.24 = bf16[8,1,24,2560]{3,2,0,1:T(8,128)(2,1)S(1)} fusion(bf16[1,2240,2560]{2,1,0:T(8,128)(2,1)} %param.13, bf16[8,24,2560]{2,1,0:T(8,128)(2,1)S(1)} %all-gather, bf16[1,2240,2560]{2,1,0:T(8,128)(2,1)} %param.12, f32[8,1,24,2240]{3,2,0,1:T(8,128)} %fusion.6), kind=kOutput, calls=%fused_computation.14 | convolution fusion | flops 4407091200 | bytes 26624000 | tf_op jit(solution)/shard_map/sjcf,jfd->sjcd/dot_general | solution.py:61
  65.3 4.6 %copy.18 = bf16[8,1,24,2560]{2,0,1,3:T(8,128)(2,1)} copy(bf16[8,1,24,2560]{3,2,0,1:T(8,128)(2,1)S(1)} %fusion.24) | data formatting | bytes 1966080
  69.8 7.3 %reshape.134 = bf16[2560,192]{1,0:T(8,128)(2,1)} reshape(bf16[2560,1,8,24]{3,2,1,0:T(8,128)(2,1)} %bitcast.105) | data formatting | bytes 1966080
  77.2 27.0 %reduce-scatter.4.cloned.1.call-done = bf16[640,192]{1,0:T(8,128)(2,1)} async-done(((bf16[2560,192]{1,0:T(8,128)(2,1)}), bf16[640,192]{1,0:T(8,128)(2,1)}) %reduce-scatter.4.cloned.1.call-update) | async-done | bytes 245776
  104.2 2.0 %reshape.135 = bf16[640,1,8,24]{3,2,1,0:T(8,128)(2,1)S(1)} reshape(bf16[640,192]{1,0:T(8,128)(2,1)} %reduce-scatter.4.cloned.1.call-done) | data formatting | bytes 491520
  106.2 1.5 %copy.19 = bf16[8,1,24,640]{3,2,0,1:T(8,128)(2,1)} copy(bf16[8,1,24,640]{2,0,1,3:T(8,128)(2,1)S(1)} %bitcast.107) | data formatting | bytes 491520
  107.7 4.6 %all-to-all-start = ((bf16[8,1,24,640]{3,2,1,0:T(8,128)(2,1)}), bf16[8,1,24,640]{3,2,1,0:T(8,128)(2,1)S(1)}, u32[]{:S(2)}, u32[]{:S(2)}) async-start(bf16[8,1,24,640]{3,2,1,0:T(8,128)(2,1)} %bitcast.35), calls=%async_computation | async-start | bytes 491520 | tf_op jit(solution)/shard_map/all_to_all | solution.py:67
  112.6 9.0 %all-to-all-done = bf16[8,1,24,640]{3,2,1,0:T(8,128)(2,1)S(1)} async-done(((bf16[8,1,24,640]{3,2,1,0:T(8,128)(2,1)}), bf16[8,1,24,640]{3,2,1,0:T(8,128)(2,1)S(1)}, u32[]{:S(2)}, u32[]{:S(2)}) %all-to-all-start) | async-done | bytes 245792 | tf_op jit(solution)/shard_map/all_to_all | solution.py:67
  121.7 0.9 gather_fusion.1
  122.6 0.9 multiply_reduce_fusion
  (38 shorter events, 1.6 us)
Async XLA Ops:
  6.5 97.6 %reduce-scatter.4.cloned.1.call-start = ((), (), s32[]{:S(2)}) async-start(), calls=%async_computation.2 | async-start | bytes 1638400
  10.6 6.0 %collective-permute-start = (bf16[1,1,24,640]{3,2,1,0:T(8,128)(2,1)S(1)}, bf16[1,1,24,640]{3,2,1,0:T(8,128)(2,1)S(1)}, u32[]{:S(2)}, u32[]{:S(2)}) collective-permute-start(bf16[1,1,24,640]{3,2,1,0:T(8,128)(2,1)S(1)} %get-tuple-element.11), channel_id=1, source_target_pairs={{0,4},{4,0},{8,12},{12,8},{16,20},{20,16},{24,28},{28,24},{1,5},{5... | collective-permute-start | bytes 92168 | tf_op jit(solution)/shard_map/ppermute | solution.py:26
  11.2 9.2 %collective-permute-start.1 = (bf16[1,1,24,640]{3,2,1,0:T(8,128)(2,1)S(1)}, bf16[1,1,24,640]{3,2,1,0:T(8,128)(2,1)S(1)}, u32[]{:S(2)}, u32[]{:S(2)}) collective-permute-start(bf16[1,1,24,640]{3,2,1,0:T(8,128)(2,1)S(1)} %get-tuple-element.10), channel_id=1, source_target_pairs={{0,8},{4,12},{8,0},{12,4},{16,24},{20,28},{24,16},{28,20},{1,9},{5... | collective-permute-start | bytes 92168 | tf_op jit(solution)/shard_map/ppermute | solution.py:26
  13.8 6.7 %collective-permute-start.2 = (bf16[1,1,24,640]{3,2,1,0:T(8,128)(2,1)S(1)}, bf16[1,1,24,640]{3,2,1,0:T(8,128)(2,1)S(1)}, u32[]{:S(2)}, u32[]{:S(2)}) collective-permute-start(bf16[1,1,24,640]{3,2,1,0:T(8,128)(2,1)S(1)} %get-tuple-element.9), channel_id=1, source_target_pairs={{0,12},{4,8},{8,4},{12,0},{16,28},{20,24},{24,20},{28,16},{1,13},{... | collective-permute-start | bytes 92168 | tf_op jit(solution)/shard_map/ppermute | solution.py:26
  13.8 6.6 %collective-permute-start.3 = (bf16[1,1,24,640]{3,2,1,0:T(8,128)(2,1)S(1)}, bf16[1,1,24,640]{3,2,1,0:T(8,128)(2,1)S(1)}, u32[]{:S(2)}, u32[]{:S(2)}) collective-permute-start(bf16[1,1,24,640]{3,2,1,0:T(8,128)(2,1)S(1)} %get-tuple-element.8), channel_id=1, source_target_pairs={{0,16},{4,20},{8,24},{12,28},{16,0},{20,4},{24,8},{28,12},{1,17},{... | collective-permute-start | bytes 92168 | tf_op jit(solution)/shard_map/ppermute | solution.py:26
  16.6 4.3 %collective-permute-start.4 = (bf16[1,1,24,640]{3,2,1,0:T(8,128)(2,1)S(1)}, bf16[1,1,24,640]{3,2,1,0:T(8,128)(2,1)S(1)}, u32[]{:S(2)}, u32[]{:S(2)}) collective-permute-start(bf16[1,1,24,640]{3,2,1,0:T(8,128)(2,1)S(1)} %get-tuple-element.7), channel_id=1, source_target_pairs={{0,20},{4,16},{8,28},{12,24},{16,4},{20,0},{24,12},{28,8},{1,21},{... | collective-permute-start | bytes 92168 | tf_op jit(solution)/shard_map/ppermute | solution.py:26
  16.6 6.3 %collective-permute-start.5 = (bf16[1,1,24,640]{3,2,1,0:T(8,128)(2,1)S(1)}, bf16[1,1,24,640]{3,2,1,0:T(8,128)(2,1)S(1)}, u32[]{:S(2)}, u32[]{:S(2)}) collective-permute-start(bf16[1,1,24,640]{3,2,1,0:T(8,128)(2,1)S(1)} %get-tuple-element.6), channel_id=1, source_target_pairs={{0,24},{4,28},{8,16},{12,20},{16,8},{20,12},{24,0},{28,4},{1,25},{... | collective-permute-start | bytes 92168 | tf_op jit(solution)/shard_map/ppermute | solution.py:26
  20.3 5.2 %collective-permute-start.6 = (bf16[1,1,24,640]{3,2,1,0:T(8,128)(2,1)S(1)}, bf16[1,1,24,640]{3,2,1,0:T(8,128)(2,1)S(1)}, u32[]{:S(2)}, u32[]{:S(2)}) collective-permute-start(bf16[1,1,24,640]{3,2,1,0:T(8,128)(2,1)S(1)} %get-tuple-element.5), channel_id=1, source_target_pairs={{0,28},{4,24},{8,20},{12,16},{16,12},{20,8},{24,4},{28,0},{1,29},{... | collective-permute-start | bytes 92168 | tf_op jit(solution)/shard_map/ppermute | solution.py:26
  77.2 35.2 %copy-start = (s32[32,4]{0,1:T(4,128)S(1)}, s32[32,4]{0,1:T(4,128)}, u32[]{:S(2)}) copy-start(s32[32,4]{0,1:T(4,128)} %param.9) | copy-start | bytes 1540
  77.2 35.4 %copy-start.1 = (f32[32,4]{0,1:T(4,128)S(1)}, f32[32,4]{0,1:T(4,128)}, u32[]{:S(2)}) copy-start(f32[32,4]{0,1:T(4,128)} %param.10) | copy-start | bytes 1540
  107.7 14.0 %all-to-all-start = ((bf16[8,1,24,640]{3,2,1,0:T(8,128)(2,1)}), bf16[8,1,24,640]{3,2,1,0:T(8,128)(2,1)S(1)}, u32[]{:S(2)}, u32[]{:S(2)}) async-start(bf16[8,1,24,640]{3,2,1,0:T(8,128)(2,1)} %bitcast.35), calls=%async_computation | async-start | bytes 491520 | tf_op jit(solution)/shard_map/all_to_all | solution.py:67
Sparse Core Ops, SparseCore 0:
  77.3 26.8 reduce-scatter.3
